TPU v7x, 32 devices: a whole 2x2x4 slice. The times are simulated.
32 devices in a mesh: fs: 4 (over z), rep: 4 (over y, x), tp: 2 (over core).
Axes of the slice: x: 2, y: 2, z: 4, core: 2. Of those that a mesh axis runs over, the one named last changes fastest.
Arguments:
- tokens_in: bfloat16 [8192, 2048], P(('fs', 'rep')), may hold values from -6 to 6
- query_two: bfloat16 [8192, 512], P(('fs', 'rep'), 'tp'), may hold values from -49 to 49
- key_two: bfloat16 [8192, 512], P(('fs', 'rep'), 'tp'), may hold values from -9 to 9
- values: bfloat16 [8192, 1024], P(('fs', 'rep'), 'tp'), may hold values from -6 to 6
- out_grad: bfloat16 [8192, 1024], P(('fs', 'rep'), 'tp'), may hold values from -6 to 6
- second_scale: float32 [8], P('tp'), may hold values from 0.3 to 0.8
- factor: bfloat16 [2048, 256], P('fs'), may hold values from -0.125 to 0.125
- weight: float32 [2048, 512], P('fs', 'tp'), may hold values from -0.6 to 0.6
- first_moment: float32 [256, 512], P('fs', 'tp'), may hold values from -135.7645 to 135.7645
- second_moment: float32 [256, 512], P('fs', 'tp'), may hold values from 5 to 8192
Outputs:
- new_weight: float32 [2048, 512], P('fs', 'tp')
- weight_copy: bfloat16 [2048, 512], P(None, 'tp')
- update_step: float32 [2048, 512], P('fs', 'tp')
- new_first: float32 [256, 512], P('fs', 'tp')
- new_second: float32 [256, 512], P('fs', 'tp')
All inputs are finite; a program needn't handle non-finite values.
Results may differ from a plain program's by a relative error of at most 0.006.
Values may be sent and summed in bfloat16 or wider, within the bound.
A program may use at most 64 MiB of HBM per device.

v0:
```python
import jax
import jax.numpy as jnp
from jax import lax
from jax.sharding import PartitionSpec as P

RANK = 256
KW = 512


by_rows = (((0,), (0,)), ((), ()))


def key_gradient(query_rows, key_rows, value_rows, grad_rows, second_scale):
    length = query_rows.shape[0]
    head_count = second_scale.shape[0]
    queries = query_rows.reshape(length, head_count, -1)
    keys_all = key_rows.reshape(length, head_count, -1)
    value_heads = value_rows.reshape(length, head_count, -1)
    grad_heads = grad_rows.reshape(length, head_count, -1)
    inv_root = queries.shape[2] ** (-0.5)
    scores = (
        jnp.einsum("qhd,khd->hqk", queries, keys_all, preferred_element_type=jnp.float32) * inv_root
    )
    positions = jnp.arange(length, dtype=jnp.int32)
    causal = positions[:, None] >= positions[None, :]
    scores = jnp.where(causal[None], scores, -1e30)
    row_peak = jnp.max(scores, axis=-1, keepdims=True)
    exps = jnp.exp(scores - row_peak)
    weights_map = exps / jnp.sum(exps, axis=-1, keepdims=True)
    attn_grad = jnp.einsum(
        "qhe,khe->hqk", grad_heads, value_heads, preferred_element_type=jnp.float32
    )
    row_inner = jnp.sum(weights_map * attn_grad, axis=-1, keepdims=True)
    score_grad = ((-second_scale)[:, None, None] * weights_map * (attn_grad - row_inner)).astype(
        jnp.bfloat16
    )
    key_grad = (
        jnp.einsum("hqk,qhd->khd", score_grad, queries, preferred_element_type=jnp.float32)
        * inv_root
    )
    return key_grad.reshape(length, -1).astype(jnp.bfloat16)


def on_device(
    tokens_in,
    query_two,
    key_two,
    values,
    out_grad,
    second_scale,
    factor,
    weight,
    first_moment,
    second_moment,
):
    key_grad = key_gradient(query_two, key_two, values, out_grad, second_scale)
    reduced = jnp.dot(
        tokens_in,
        lax.all_gather(factor, "fs", axis=0, tiled=True),
        preferred_element_type=jnp.float32,
    )
    reduced_high = reduced.astype(jnp.bfloat16)
    reduced_low = (reduced - reduced_high.astype(jnp.float32)).astype(jnp.bfloat16)
    first_part = lax.dot_general(
        reduced_high, key_grad, by_rows, preferred_element_type=jnp.float32
    )
    proj_part = lax.psum_scatter(
        first_part
        + lax.dot_general(reduced_low, key_grad, by_rows, preferred_element_type=jnp.float32),
        "fs",
        scatter_dimension=0,
        tiled=True,
    )
    projected = lax.psum(proj_part, "rep")
    new_first = 0.9 * first_moment + 0.1 * projected
    new_second = 0.95 * second_moment + 0.05 * projected * projected
    direction = (new_first / (jnp.sqrt(new_second) + 1e-08)).astype(jnp.bfloat16)
    gathered = lax.all_gather(direction, "fs", axis=0, tiled=True)
    squares = lax.psum(jnp.sum(jnp.square(direction.astype(jnp.float32))), ("fs", "tp"))
    update_step = jnp.dot(factor, gathered, preferred_element_type=jnp.float32) * lax.rsqrt(
        squares / (RANK * KW) + 1e-06
    )
    new_weight = weight - 0.1 * update_step
    copies = lax.all_gather(new_weight.astype(jnp.bfloat16), "fs", axis=0, tiled=True)
    return (new_weight, copies, update_step, new_first, new_second)


def solution(mesh):
    in_specs = (
        P(("fs", "rep"), None),
        P(("fs", "rep"), "tp"),
        P(("fs", "rep"), "tp"),
        P(("fs", "rep"), "tp"),
        P(("fs", "rep"), "tp"),
        P("tp"),
        P("fs", None),
        P("fs", "tp"),
        P("fs", "tp"),
        P("fs", "tp"),
    )
    out_specs = (P("fs", "tp"), P(None, "tp"), P("fs", "tp"), P("fs", "tp"), P("fs", "tp"))
    return jax.shard_map(
        on_device, mesh=mesh, in_specs=in_specs, out_specs=out_specs, check_vma=False
    )
```

profile of v0, /device:TPU:9, one launch (start us, length us, event | category | flops | bytes accessed | tf_op | source)
XLA Modules:
  0.0 169.5 jit_solution(17803742306093832055)
XLA Ops:
  7.2 0.0 copy-start
  7.2 0.0 all-gather.3.cloned.1.call-start
  7.2 0.7 all-gather.3.cloned.1.call-update
  7.9 0.0 reduce-scatter.2.cloned.1.call-start
  8.0 1.1 copy.25
  9.1 1.1 copy.26
  10.2 0.7 neg.3
  10.8 0.1 iota_compare_fusion
  10.9 3.8 %fusion.13 = f32[4,512,512]{1,2,0:T(8,128)} fusion(bf16[512,512]{1,0:T(8,128)(2,1)} %param.13, bf16[512,512]{1,0:T(8,128)(2,1)} %param.14), kind=kOutput, calls=%fused_computation.20 | convolution fusion | flops 268435456 | bytes 5242880 | tf_op jit(solution)/shard_map/qhe,khe->hqk/dot_general | solution.py:30
  14.7 6.6 %multiply_reduce_fusion = (f32[4,512]{1,0:T(4,128)S(1)}, f32[4,512,512]{1,2,0:T(8,128)}) fusion(f32[4,512,512]{1,2,0:T(8,128)} %fusion.13, pred[512,512]{0,1:T(8,128)(4,1)S(1)} %iota_compare_fusion, bf16[512,4,64]{0,2,1:T(8,128)(2,1)S(1)} %bitcast.34, bf16[512,4,64]{0,2,1:T(8,128)(2,1)S(1)} %bitcast.36), kind=kOutput, calls=%fused_computation.3 | convolution fusion | flops 140512256 | bytes 9183232 | tf_op jit(solution)/shard_map/div | solution.py:29
  21.4 4.3 %fusion.12 = bf16[4,512,64]{1,2,0:T(8,128)(2,1)S(1)} fusion(bf16[512,4,64]{0,2,1:T(8,128)(2,1)S(1)} %bitcast.35, f32[4,512,512]{1,2,0:T(8,128)} %fusion.13, f32[4,512,512]{1,2,0:T(8,128)} %get-tuple-element.22, f32[4,512]{1,0:T(4,128)S(1)} %get-tuple-element.21, f32[4]{0:T(128)S(1)} %neg.3), kind=kOutput, calls=%fused_computation.17 | convolution fusion | flops 138674176 | bytes 8921104 | tf_op jit(solution)/shard_map/hqk,qhd->khd/dot_general | solution.py:38
  25.7 0.0 copy-start.2
  25.7 0.0 copy-start.3
  25.7 0.0 copy-start.1
  25.7 12.2 %all-gather.3.cloned.1.call-done = bf16[2048,256]{1,0:T(8,128)(2,1)} async-done(((bf16[512,256]{1,0:T(8,128)(2,1)}), bf16[2048,256]{1,0:T(8,128)(2,1)}) %all-gather.3.cloned.1.call-update) | async-done | bytes 1048592 | tf_op jit(solution)/shard_map/all_gather | solution.py:59
  37.9 0.0 copy-done
  37.9 1.9 %fusion.30 = f32[512,256]{1,0:T(8,128)S(1)} fusion(bf16[512,2048]{1,0:T(8,128)(2,1)S(1)} %copy-done, bf16[2048,256]{1,0:T(8,128)(2,1)} %all-gather.3.cloned.1.call-done), kind=kOutput, calls=%fused_computation.39 | convolution fusion | flops 536870912 | bytes 3670016 | tf_op jit(solution)/shard_map/dot_general | solution.py:57
  39.8 0.3 fusion.21
  40.1 1.0 convolution_add_fusion
  41.1 0.0 reduce-scatter.2.cloned.1.call-update
  41.1 0.0 all-reduce.2.cloned.1.call-start
  41.2 15.6 %reduce-scatter.2.cloned.1.call-done = f32[64,256]{1,0:T(8,128)} async-done(((f32[256,256]{1,0:T(8,128)}), f32[64,256]{1,0:T(8,128)}) %reduce-scatter.2.cloned.1.call-update) | async-done | bytes 65552 | tf_op jit(solution)/shard_map/reduce_scatter | solution.py:67
  56.8 0.0 all-reduce.2.cloned.1.call-update
  56.8 0.0 all-gather.5.cloned.1.call-start
  56.9 1.2 copy.30
  58.1 45.9 %all-reduce.2.cloned.1.call-done = f32[64,256]{1,0:T(8,128)} async-done(((f32[64,256]{1,0:T(8,128)}), f32[64,256]{1,0:T(8,128)}) %all-reduce.2.cloned.1.call-update) | async-done | bytes 65552 | tf_op jit(solution)/shard_map/psum | solution.py:74
  104.0 0.0 copy-done.2
  104.0 0.0 copy-done.3
  104.0 2.1 %multiply_reduce_fusion.1 = (f32[]{:T(128)}, bf16[64,256]{1,0:T(8,128)(2,1)S(1)}, f32[64,256]{1,0:T(8,128)}, f32[64,256]{1,0:T(8,128)}) fusion(f32[64,256]{1,0:T(8,128)} %all-reduce.2.cloned.1.call-done, f32[64,256]{1,0:T(8,128)S(1)} %copy-done.2, f32[64,256]{1,0:T(8,128)S(1)} %copy-done.3), kind=kLoop, calls=%fused_computation.33 | loop fusion | flops 212991 | bytes 360452 | tf_op jit(solution)/shard_map/reduce_sum | solution.py:79
  106.2 10.5 %all_gather.10 = bf16[256,256]{1,0:T(8,128)(2,1)S(1)} all-gather(bf16[64,256]{1,0:T(8,128)(2,1)S(1)} %get-tuple-element.18), channel_id=1, replica_groups=mesh['fs'=4,'rep'=4,'tp'=2] {'fs'}, dimensions={0}, use_global_device_ids=true | all-gather | bytes 163840 | tf_op jit(solution)/shard_map/all_gather | solution.py:78
  116.7 14.3 %psum.15 = f32[]{:T(128)} all-reduce(f32[]{:T(128)} %get-tuple-element.17), channel_id=1, replica_groups=mesh['fs'=4,'rep'=4,'tp'=2] {'fs','tp'}, use_global_device_ids=true, to_apply=%region_6.7 | all-reduce | flops 1 | bytes 8 | tf_op jit(solution)/shard_map/psum | solution.py:79
  131.7 0.0 copy-done.1
  131.7 1.2 fusion.26
  132.8 0.0 all-gather.5.cloned.1.call-update
  132.9 2.0 %copy.31 = f32[512,256]{1,0:T(8,128)} copy(f32[512,256]{0,1:T(8,128)} %get-tuple-element.16) | data formatting | bytes 1048576
  134.9 1.0 copy.33
  135.9 24.8 %all-gather.5.cloned.1.call-done = bf16[2048,256]{0,1:T(8,128)(2,1)} async-done(((bf16[512,256]{0,1:T(8,128)(2,1)}), bf16[2048,256]{0,1:T(8,128)(2,1)}) %all-gather.5.cloned.1.call-update) | async-done | bytes 1048592 | tf_op jit(solution)/shard_map/all_gather | solution.py:84
  160.7 2.3 %copy.32 = bf16[2048,256]{1,0:T(8,128)(2,1)} copy(bf16[2048,256]{0,1:T(8,128)(2,1)} %all-gather.5.cloned.1.call-done) | data formatting | bytes 2097152
Async XLA Ops:
  7.2 30.7 %copy-start = (bf16[512,2048]{1,0:T(8,128)(2,1)S(1)}, bf16[512,2048]{1,0:T(8,128)(2,1)}, u32[]{:S(2)}) copy-start(bf16[512,2048]{1,0:T(8,128)(2,1)} %param.10) | copy-start | bytes 6291460
  7.2 30.7 %all-gather.3.cloned.1.call-start = ((), (), s32[]{:S(2)}) async-start(), calls=%async_computation.1 | async-start | bytes 1310720 | tf_op jit(solution)/shard_map/all_gather | solution.py:59
  7.9 48.9 %reduce-scatter.2.cloned.1.call-start = ((), (), s32[]{:S(2)}) async-start(), calls=%async_computation.2 | async-start | bytes 327680 | tf_op jit(solution)/shard_map/reduce_scatter | solution.py:67
  25.7 78.4 %copy-start.2 = (f32[64,256]{1,0:T(8,128)S(1)}, f32[64,256]{1,0:T(8,128)}, u32[]{:S(2)}) copy-start(f32[64,256]{1,0:T(8,128)} %param.19) | copy-start | bytes 196612
  25.7 78.3 %copy-start.3 = (f32[64,256]{1,0:T(8,128)S(1)}, f32[64,256]{1,0:T(8,128)}, u32[]{:S(2)}) copy-start(f32[64,256]{1,0:T(8,128)} %param.18) | copy-start | bytes 196612
  25.7 106.0 %copy-start.1 = (bf16[512,256]{1,0:T(8,128)(2,1)S(1)}, bf16[512,256]{1,0:T(8,128)(2,1)}, u32[]{:S(2)}) copy-start(bf16[512,256]{1,0:T(8,128)(2,1)} %param.16) | copy-start | bytes 786436
  41.1 62.9 %all-reduce.2.cloned.1.call-start = ((), (), s32[]{:S(2)}) async-start(), calls=%async_computation.3 | async-start | bytes 131072 | tf_op jit(solution)/shard_map/psum | solution.py:74
  56.8 103.8 %all-gather.5.cloned.1.call-start = ((), (), s32[]{:S(2)}) async-start(), calls=%async_computation.4 | async-start | bytes 1310720 | tf_op jit(solution)/shard_map/all_gather | solution.py:84
Sparse Core Ops, SparseCore 0:
  9.6 28.2 all-gather.2
  41.2 15.5 reduce-scatter.1
  59.7 44.3 all-reduce.1
  133.0 27.6 all-gather.4
where the time goes:
time: 172 us; the launch traced here: 169 us
  waiting for transfers between devices  99.2 us (58%)
  blocking collectives  24.8 us (14%)
  matrix products  19.1 us (11%)
  between operations  14.5 us (8%)
  local copies, waits for them, and re-layouts  8.74 us (5%)
  other arithmetic  2.86 us (2%)
    psum x1, waiting for transfers between devices, on_device(): projected = lax.psum(proj_part, 'rep')  45.9 us
    all_gather x1, waiting for transfers between devices, on_device(): lax.all_gather(new_weight.astype(jnp.bfloat16), 'fs', axis=0, tiled=True)  24.8 us
    reduce_scatter x1, waiting for transfers between devices, on_device(): lax.psum_scatter(first_part + lax.dot_general(reduced_low, key_grad, by_r...  15.6 us
    psum x1, blocking collectives, on_device(): lax.psum(jnp.sum(jnp.square(direction.astype(jnp.float32))), ('fs', 'tp'))  14.3 us
    all_gather x1, waiting for transfers between devices, on_device(): lax.all_gather(factor, 'fs', axis=0, tiled=True)  12.2 us
    all_gather x1, blocking collectives, on_device(): gathered = lax.all_gather(direction, 'fs', axis=0, tiled=True)  10.5 us
    unnamed x14, local copies, waits for them, and re-layouts  8.74 us
    div x1, matrix products, key_gradient(): weights_map = exps / jnp.sum(exps, axis=-1, keepdims=True)  6.63 us
  transfers between devices with their start and end apart: 4, of which 4 were waited for; matrix products, arithmetic and copies ran while one was open for 13% of the time, Pallas kernels for 0%

commit v1 on v0

v1 whole, which is shorter than its diff:
```python
import functools

import jax
import jax.numpy as jnp
from jax import lax
from jax.experimental import pallas as pl
from jax.experimental.pallas import tpu as pltpu
from jax.sharding import PartitionSpec as P

MESH = pl.DeviceIdType.MESH
LANES = 128
NT = (((1,), (1,)), ((), ()))
TN = (((0,), (0,)), ((), ()))


def attention_pair(pair, q_v, k_v, v_v, g_v, scale_ref, acc, kgb, head_width):
    length = q_v.shape[0]
    per = LANES // head_width
    block = min(LANES, length)
    cols = slice(pair * LANES, (pair + 1) * LANES)
    value_width = v_v.shape[1] // (q_v.shape[1] // head_width)
    lane = lax.broadcasted_iota(jnp.int32, (length, LANES), 1)
    tri = lax.broadcasted_iota(jnp.int32, (block, block), 0) <= lax.broadcasted_iota(
        jnp.int32, (block, block), 1
    )
    for inner_head in range(per):
        head = pair * per + inner_head
        in_head = (lane >= inner_head * head_width) & (lane < (inner_head + 1) * head_width)
        queries = jnp.where(in_head, q_v[:, cols].astype(jnp.float32) * head_width ** (-0.5), 0.0)
        queries = queries.astype(jnp.bfloat16)
        vcols = slice(head * value_width, (head + 1) * value_width)
        scale = scale_ref[head]
        for at in reversed(range(length // block)):
            keys_to = (at + 1) * block
            rows = slice(at * block, keys_to)
            qb = queries[rows]
            s = lax.dot_general(k_v[:keys_to, cols], qb, NT, preferred_element_type=jnp.float32)
            last = jnp.where(tri, s[at * block :], -1e30)
            s = last if at == 0 else jnp.concatenate([s[: at * block], last], axis=0)
            e = jnp.exp(s - jnp.max(s, axis=0, keepdims=True))
            inv = 1.0 / jnp.sum(e, axis=0, keepdims=True)
            a = lax.dot_general(
                v_v[:keys_to, vcols], g_v[rows, vcols], NT, preferred_element_type=jnp.float32
            )
            row_inner = jnp.sum(e * a, axis=0, keepdims=True) * inv
            sg = (e * (a - row_inner) * (-scale * inv)).astype(jnp.bfloat16)
            add = jnp.dot(sg, qb, preferred_element_type=jnp.float32)
            if inner_head == 0 and at == length // block - 1:
                acc[...] = add
            else:
                acc[:keys_to] += add
    kgb[:, cols] = acc[...].astype(jnp.bfloat16)


def main_kernel(
    fs, rep, tp, head_width,
    scale_ref, tok_h, q_h, k_h, v_h, g_h, factor_h, weight_h, first_h, second_h,
    fac, wbf, dirs, proj, sq_out,
    tok, q_v, k_v, v_v, g_v, wq, wsend, fm, sm, acc, kgb, red, psend, precv, sq_own, sq_in,
    ld, fac_s, fac_r, par_s, par_r, w_s, w_r, wf_s, wf_r, pc_s, pc_r, dr_s, dr_r, pj_s, pj_r, sq_s, sq_r,
):
    n = fs * rep
    z, r, c = lax.axis_index("fs"), lax.axis_index("rep"), lax.axis_index("tp")
    me = z * rep + r
    other = lax.rem(c + 1, tp)
    partner = {"fs": z, "rep": r, "tp": other}
    half = fac.shape[2] // tp
    my_cols = pl.ds(pl.multiple_of(c * half, half), half)
    his_cols = pl.ds(pl.multiple_of(other * half, half), half)

    def remote(src, dst, send, recv, device):
        return pltpu.make_async_remote_copy(
            src_ref=src, dst_ref=dst, send_sem=send, recv_sem=recv, device_id=device, device_id_type=MESH
        )

    def fs_dev(i):
        return {"fs": i, "rep": r, "tp": c}

    def rep_dev(i):
        return {"fs": z, "rep": i, "tp": c}

    def any_dev(i):
        return {"fs": i // rep, "rep": lax.rem(i, rep), "tp": c}

    def each(count, body):
        def step(d, carry):
            body(d)
            return carry

        lax.fori_loop(1, count, step, 0)

    barrier = pltpu.get_barrier_semaphore()
    pl.semaphore_signal(barrier, inc=1, device_id=partner, device_id_type=MESH)

    def greet(d):
        pl.semaphore_signal(barrier, inc=1, device_id=any_dev(lax.rem(me + d, n)), device_id_type=MESH)

    each(n, greet)

    loads = [
        pltpu.make_async_copy(src, dst, ld.at[i])
        for i, (src, dst) in enumerate(
            [
                (factor_h, fac.at[z]), (weight_h.at[r], wq), (q_h, q_v), (k_h, k_v), (v_h, v_v), (g_h, g_v),
                (tok_h, tok), (first_h.at[r], fm), (second_h.at[r], sm),
            ]
        )
    ]
    for load in loads:
        load.start()
    loads[1].wait()
    wsend[...] = wq[...].astype(jnp.bfloat16)
    loads[0].wait()
    pl.semaphore_wait(barrier, n)

    def fac_copy(slot, sem, to):
        part = fac.at[slot, :, my_cols]
        return remote(part, part, fac_s.at[sem], fac_r.at[slot], fs_dev(to))

    def send_fac(d):
        fac_copy(z, d, lax.rem(z + d, fs)).start()

    each(fs, send_fac)

    def w_copy(slot, sem, to):
        return remote(wsend, wbf.at[slot, r], w_s.at[sem], w_r.at[slot], fs_dev(to))

    def send_w(d):
        w_copy(z, d, lax.rem(z + d, fs)).start()

    each(fs, send_w)

    for i in range(2, 6):
        loads[i].wait()
    for pair in range(q_v.shape[1] // LANES):
        attention_pair(pair, q_v, k_v, v_v, g_v, scale_ref, acc, kgb, head_width)
    for i in range(6, 9):
        loads[i].wait()

    by_shard = fac.shape[1] % LANES == 0

    def tokens_of(j):
        return tok[:, pl.ds(pl.multiple_of(j * fac.shape[1], LANES), fac.shape[1])]

    if by_shard:
        red[...] = jnp.dot(tokens_of(z), fac[z], preferred_element_type=jnp.float32)

    def par_copy(slot, cols):
        part = fac.at[slot, :, cols]
        return remote(part, part, par_s.at[slot], par_r.at[slot], partner)

    def forward_fac(d):
        src = lax.rem(z + d, fs)
        fac_copy(src, d, src).wait_recv()
        par_copy(src, my_cols).start()

    each(fs, forward_fac)

    def use_fac(d):
        src = lax.rem(z + d, fs)
        par_copy(src, his_cols).wait_recv()
        if by_shard:
            red[...] += jnp.dot(tokens_of(src), fac[src], preferred_element_type=jnp.float32)

    each(fs, use_fac)
    if not by_shard:
        whole = jnp.concatenate([fac[j] for j in range(fs)], axis=0)
        red[...] = jnp.dot(tok[...], whole, preferred_element_type=jnp.float32)

    partial = lax.dot_general(
        red[...].astype(jnp.bfloat16), kgb[...], TN, preferred_element_type=jnp.float32
    )
    piece = psend.shape[1]
    for i in range(n):
        psend[i] = partial[i * piece : (i + 1) * piece].astype(jnp.bfloat16)

    def pc_copy(part, slot, sem, to):
        return remote(psend.at[part], precv.at[slot], pc_s.at[sem], pc_r.at[slot], any_dev(to))

    def send_piece(d):
        to = lax.rem(me + d, n)
        pc_copy(to, me, d, to).start()

    each(n, send_piece)

    def wf_copy(slot, lane, sem, to):
        part = wbf.at[slot, lane]
        return remote(part, part, wf_s.at[slot, sem], wf_r.at[slot, lane], rep_dev(to))

    def relay_w(d):
        src = lax.rem(z + d, fs)
        w_copy(src, d, src).wait_recv()
        each(rep, lambda k: wf_copy(src, r, k, lax.rem(r + k, rep)).start())

    each(fs, relay_w)

    def wait_piece(d):
        src = lax.rem(me + d, n)
        pc_copy(src, src, d, src).wait_recv()

    each(n, wait_piece)
    precv[me] = psend[me]
    total = jnp.sum(precv[...].astype(jnp.float32), axis=0)
    first = 0.9 * fm[...] + 0.1 * total
    second = 0.95 * sm[...] + 0.05 * total * total
    dirs[me] = (first / (jnp.sqrt(second) + 1e-08)).astype(jnp.bfloat16)
    proj[r] = total

    def dr_copy(slot, sem, to):
        part = dirs.at[slot]
        return remote(part, part, dr_s.at[sem], dr_r.at[slot], any_dev(to))

    def pj_copy(slot, sem, to):
        part = proj.at[slot]
        return remote(part, part, pj_s.at[sem], pj_r.at[slot], rep_dev(to))

    each(n, lambda d: dr_copy(me, d, lax.rem(me + d, n)).start())
    each(rep, lambda d: pj_copy(r, d, lax.rem(r + d, rep)).start())

    def wait_dir(d):
        src = lax.rem(me + d, n)
        dr_copy(src, d, src).wait_recv()

    each(n, wait_dir)
    wide = dirs[...].astype(jnp.float32)
    sq_own[...] = jnp.full(sq_own.shape, jnp.sum(wide * wide), jnp.float32)
    sq_copy = remote(sq_own, sq_in, sq_s, sq_r, partner)
    sq_copy.start()

    def wait_proj(d):
        src = lax.rem(r + d, rep)
        pj_copy(src, d, src).wait_recv()

    each(rep, wait_proj)

    def wait_relay(d):
        src = lax.rem(z + d, fs)

        def inner(k):
            lane = lax.rem(r + k, rep)
            wf_copy(src, lane, k, lane).wait_recv()

        each(rep, inner)

    each(fs, wait_relay)

    def wait_sends_fs(d):
        src = lax.rem(z + d, fs)
        fac_copy(z, d, src).wait_send()
        w_copy(z, d, src).wait_send()
        par_copy(src, my_cols).wait_send()
        each(rep, lambda k: wf_copy(src, r, k, lax.rem(r + k, rep)).wait_send())

    each(fs, wait_sends_fs)

    def wait_sends_all(d):
        to = lax.rem(me + d, n)
        pc_copy(to, me, d, to).wait_send()
        dr_copy(me, d, to).wait_send()

    each(n, wait_sends_all)
    each(rep, lambda d: pj_copy(r, d, lax.rem(r + d, rep)).wait_send())
    sq_copy.wait()
    sq_out[...] = sq_own[...] + sq_in[...]


def end_kernel(
    fs, entries,
    sq, factor, direction, fac, wbf, weight, proj, fm, sm,
    new_weight, copies, update, new_first, new_second,
):
    z = lax.axis_index("fs")
    rows = factor.shape[0]
    ratio = lax.rsqrt(sq[0:1, 0:1] / entries + 1e-06)
    own = jnp.dot(factor[...], direction[...], preferred_element_type=jnp.float32) * ratio
    update[...] = own
    changed = weight[...] - 0.1 * own
    new_weight[...] = changed
    copies[pl.ds(pl.multiple_of(z * rows, rows), rows), :] = changed.astype(jnp.bfloat16)
    for d in range(1, fs):
        at = pl.ds(pl.multiple_of(lax.rem(z + d, fs) * rows, rows), rows)
        step = jnp.dot(fac[at, :], direction[...], preferred_element_type=jnp.float32) * ratio
        copies[at, :] = (wbf[at, :].astype(jnp.float32) - 0.1 * step).astype(jnp.bfloat16)
    total = proj[...]
    new_first[...] = 0.9 * fm[...] + 0.1 * total
    new_second[...] = 0.95 * sm[...] + 0.05 * total * total


def on_device(
    fs, rep, tp,
    tokens_in, query_two, key_two, values, out_grad, second_scale, factor, weight, first_moment, second_moment,
):
    n = fs * rep
    length, width = query_two.shape
    head_width = width // second_scale.shape[0]
    rows, rank = factor.shape
    own_rows = first_moment.shape[0]
    piece = own_rows // rep
    w_rows = rows // rep
    f32, bf16 = jnp.float32, jnp.bfloat16
    any_spec = pl.BlockSpec(memory_space=pl.ANY)
    vmem = pl.BlockSpec(memory_space=pltpu.VMEM)
    dma = pltpu.SemaphoreType.DMA
    fac, wbf, dirs, proj, sq = pl.pallas_call(
        functools.partial(main_kernel, fs, rep, tp, head_width),
        out_shape=(
            jax.ShapeDtypeStruct((fs, rows, rank), bf16),
            jax.ShapeDtypeStruct((fs, rep, w_rows, width), bf16),
            jax.ShapeDtypeStruct((n, piece, width), bf16),
            jax.ShapeDtypeStruct((rep, piece, width), f32),
            jax.ShapeDtypeStruct((8, LANES), f32),
        ),
        in_specs=[pl.BlockSpec(memory_space=pltpu.SMEM)] + [any_spec] * 9,
        out_specs=(vmem,) * 5,
        scratch_shapes=[
            pltpu.VMEM(tokens_in.shape, bf16),
            pltpu.VMEM(query_two.shape, bf16),
            pltpu.VMEM(key_two.shape, bf16),
            pltpu.VMEM(values.shape, bf16),
            pltpu.VMEM(out_grad.shape, bf16),
            pltpu.VMEM((w_rows, width), f32),
            pltpu.VMEM((w_rows, width), bf16),
            pltpu.VMEM((piece, width), f32),
            pltpu.VMEM((piece, width), f32),
            pltpu.VMEM((length, LANES), f32),
            pltpu.VMEM((length, width), bf16),
            pltpu.VMEM((length, rank), f32),
            pltpu.VMEM((n, piece, width), bf16),
            pltpu.VMEM((n, piece, width), bf16),
            pltpu.VMEM((8, LANES), f32),
            pltpu.VMEM((8, LANES), f32),
            dma((9,)),
            dma((fs,)), dma((fs,)),
            dma((fs,)), dma((fs,)),
            dma((fs,)), dma((fs,)),
            dma((fs, rep)), dma((fs, rep)),
            dma((n,)), dma((n,)),
            dma((n,)), dma((n,)),
            dma((rep,)), dma((rep,)),
            dma, dma,
        ],
        compiler_params=pltpu.CompilerParams(
            collective_id=0, has_side_effects=True, vmem_limit_bytes=48 * 1024 * 1024
        ),
        name="main_kernel",
    )(
        second_scale, tokens_in, query_two, key_two, values, out_grad, factor,
        weight.reshape(rep, w_rows, width),
        first_moment.reshape(rep, piece, width),
        second_moment.reshape(rep, piece, width),
    )
    return pl.pallas_call(
        functools.partial(end_kernel, fs, float(rank * width * tp)),
        out_shape=(
            jax.ShapeDtypeStruct(weight.shape, f32),
            jax.ShapeDtypeStruct((fs * rows, width), bf16),
            jax.ShapeDtypeStruct(weight.shape, f32),
            jax.ShapeDtypeStruct(first_moment.shape, f32),
            jax.ShapeDtypeStruct(first_moment.shape, f32),
        ),
        in_specs=[vmem] * 9,
        out_specs=(vmem,) * 5,
        compiler_params=pltpu.CompilerParams(vmem_limit_bytes=32 * 1024 * 1024),
        name="end_kernel",
    )(
        sq, factor, dirs.reshape(n * piece, width), fac.reshape(fs * rows, rank),
        wbf.reshape(fs * rows, width), weight, proj.reshape(own_rows, width), first_moment, second_moment,
    )


def solution(mesh):
    sizes = (mesh.shape["fs"], mesh.shape["rep"], mesh.shape["tp"])
    in_specs = (
        P(("fs", "rep"), None),
        P(("fs", "rep"), "tp"),
        P(("fs", "rep"), "tp"),
        P(("fs", "rep"), "tp"),
        P(("fs", "rep"), "tp"),
        P("tp"),
        P("fs", None),
        P("fs", "tp"),
        P("fs", "tp"),
        P("fs", "tp"),
    )
    out_specs = (P("fs", "tp"), P(None, "tp"), P("fs", "tp"), P("fs", "tp"), P("fs", "tp"))
    return jax.shard_map(
        functools.partial(on_device, *sizes),
        mesh=mesh, in_specs=in_specs, out_specs=out_specs, check_vma=False,
    )
```

time: 172 us -> 49.9 us (0.29)
  waiting for transfers between devices: 99.2 us -> 0 us
  Pallas kernels: 0 us -> 39.9 us
  blocking collectives: 24.8 us -> 0 us
  matrix products: 19.1 us -> 0 us
  between operations: 14.5 us -> 0.66 us
  other arithmetic: 2.86 us -> 0 us
    psum x1 -> x0, waiting for transfers between devices: 45.9 us -> none  [on_device(): projected = lax.psum(proj_part, 'rep')]
    pallas_call x0 -> x2, Pallas kernels: none -> 39.9 us  [the longest x1 38.3 us: on_device(): pl.pallas_call(functools.partial(main_kernel, fs, rep, tp, head_width), o...]
    all_gather x2 -> x0, waiting for transfers between devices: 36.9 us -> none  [the longest x1 24.8 us: on_device(): lax.all_gather(new_weight.astype(jnp.bfloat16), 'fs', axis=0, tiled=True)]
    reduce_scatter x1 -> x0, waiting for transfers between devices: 15.6 us -> none  [on_device(): lax.psum_scatter(first_part + lax.dot_general(reduced_low, key_grad, by_r...]
    psum x1 -> x0, blocking collectives: 14.3 us -> none  [on_device(): lax.psum(jnp.sum(jnp.square(direction.astype(jnp.float32))), ('fs', 'tp'))]
    dot_general x6 -> x0, matrix products: 12.5 us -> none  [the longest x1 4.31 us: key_gradient(): jnp.einsum('hqk,qhd->khd', score_grad, queries, preferred_element_type=jn...]
    all_gather x1 -> x0, blocking collectives: 10.5 us -> none  [on_device(): gathered = lax.all_gather(direction, 'fs', axis=0, tiled=True)]
    div x1 -> x0, matrix products: 6.63 us -> none  [key_gradient(): weights_map = exps / jnp.sum(exps, axis=-1, keepdims=True)]
  transfers between devices with their start and end apart: 4 -> 0, of which waited for: 4 -> 0; matrix products, arithmetic and copies ran while one was open for 13% -> 0% of each run, Pallas kernels for 0% -> 0%
where the time goes in v1:
time: 49.9 us; the launch traced here: 48.9 us
  Pallas kernels  39.9 us (80%)
  local copies, waits for them, and re-layouts  8.3 us (17%)
  between operations  0.66 us (1%)
    pallas_call x1, Pallas kernels, on_device(): pl.pallas_call(functools.partial(main_kernel, fs, rep, tp, head_width), o...  38.3 us
    unnamed x18, local copies, waits for them, and re-layouts  8.3 us
    pallas_call x1, Pallas kernels, on_device(): pl.pallas_call(functools.partial(end_kernel, fs, float(rank * width * tp)...  1.68 us

profile of v1, /device:TPU:9, one launch (start us, length us, event | category | flops | bytes accessed | tf_op | source)
XLA Modules:
  0.0 48.9 jit_solution(5662820793824886989)
XLA Ops:
  0.6 0.0 copy-start
  0.6 1.0 %copy-done = f32[512,256]{1,0:T(8,128)S(1)} copy-done((f32[512,256]{1,0:T(8,128)S(1)}, f32[512,256]{1,0:T(8,128)}, u32[]{:S(2)}) %copy-start) | copy-done | bytes 524312
  1.7 0.0 copy-start.1
  1.7 0.9 %copy-done.1 = bf16[512,256]{1,0:T(8,128)(2,1)S(1)} copy-done((bf16[512,256]{1,0:T(8,128)(2,1)S(1)}, bf16[512,256]{1,0:T(8,128)(2,1)}, u32[]{:S(2)}) %copy-start.1) | copy-done | bytes 262168
  2.6 0.0 copy-start.2
  2.6 1.0 %copy-done.2 = bf16[512,512]{1,0:T(8,128)(2,1)S(1)} copy-done((bf16[512,512]{1,0:T(8,128)(2,1)S(1)}, bf16[512,512]{1,0:T(8,128)(2,1)}, u32[]{:S(2)}) %copy-start.2) | copy-done | bytes 524312
  3.7 0.0 copy-start.3
  3.7 1.0 %copy-done.3 = bf16[512,512]{1,0:T(8,128)(2,1)S(1)} copy-done((bf16[512,512]{1,0:T(8,128)(2,1)S(1)}, bf16[512,512]{1,0:T(8,128)(2,1)}, u32[]{:S(2)}) %copy-start.3) | copy-done | bytes 524312
  4.7 0.0 copy-start.4
  4.7 0.8 %copy-done.4 = f32[64,256]{1,0:T(8,128)S(1)} copy-done((f32[64,256]{1,0:T(8,128)S(1)}, f32[64,256]{1,0:T(8,128)}, u32[]{:S(2)}) %copy-start.4) | copy-done | bytes 65560
  5.6 0.0 copy-start.5
  5.6 0.8 %copy-done.5 = f32[64,256]{1,0:T(8,128)S(1)} copy-done((f32[64,256]{1,0:T(8,128)S(1)}, f32[64,256]{1,0:T(8,128)}, u32[]{:S(2)}) %copy-start.5) | copy-done | bytes 65560
  6.4 0.0 copy-start.6
  6.4 0.9 %copy-done.6 = bf16[512,256]{1,0:T(8,128)(2,1)S(1)} copy-done((bf16[512,256]{1,0:T(8,128)(2,1)S(1)}, bf16[512,256]{1,0:T(8,128)(2,1)}, u32[]{:S(2)}) %copy-start.6) | copy-done | bytes 262168
  7.3 0.0 copy-start.7
  7.3 0.9 %copy-done.7 = bf16[512,256]{1,0:T(8,128)(2,1)S(1)} copy-done((bf16[512,256]{1,0:T(8,128)(2,1)S(1)}, bf16[512,256]{1,0:T(8,128)(2,1)}, u32[]{:S(2)}) %copy-start.7) | copy-done | bytes 262168
  8.3 0.0 copy-start.8
  8.3 0.7 %copy-done.8 = f32[4]{0:T(128)S(1)} copy-done((f32[4]{0:T(128)S(1)}, f32[4]{0:T(128)}, u32[]{:S(2)}) %copy-start.8) | copy-done | bytes 40
  8.9 38.3 %main_kernel.1 = (bf16[4,512,256]{2,1,0:T(8,128)(2,1)S(1)}, bf16[4,4,128,256]{3,2,1,0:T(8,128)(2,1)S(1)}, bf16[16,16,256]{2,1,0:T(8,128)(2,1)S(1)}, f32[4,16,256]{2,1,0:T(8,128)S(1)}, f32[8,128]{1,0:T(8,128)S(1)}) custom-call(f32[4]{0:T(128)S(1)} %copy-done.8, bf16[512,2048]{1,0:T(8,128)(2,1)} %tok_h.1, bf16[512,256]{1,0:T(8,128)(2,1)S(1)} %copy-done.6, ...), custom_call_target="tpu_custom_call" | custom-call | tf_op jit(solution)/shard_map/main_kernel/pallas_call | solution.py:304
  47.2 1.7 %end_kernel.1 = (f32[512,256]{1,0:T(8,128)}, bf16[2048,256]{1,0:T(8,128)(2,1)}, f32[512,256]{1,0:T(8,128)}, f32[64,256]{1,0:T(8,128)}, f32[64,256]{1,0:T(8,128)}) custom-call(f32[8,128]{1,0:T(8,128)S(1)} %get-tuple-element.10.sq, bf16[512,256]{1,0:T(8,128)(2,1)S(1)} %copy-done.1, bf16[256,256]{1,0:T(8,128)(2,1)S(1)} %bitcast.12, ...), custom_call_target="tpu_custom_call" | custom-call | tf_op jit(solution)/shard_map/end_kernel/pallas_call | solution.py:352
Async XLA Ops:
  0.6 1.0 %copy-start = (f32[512,256]{1,0:T(8,128)S(1)}, f32[512,256]{1,0:T(8,128)}, u32[]{:S(2)}) copy-start(f32[512,256]{1,0:T(8,128)} %weight.1) | copy-start | bytes 1572868
  1.7 0.9 %copy-start.1 = (bf16[512,256]{1,0:T(8,128)(2,1)S(1)}, bf16[512,256]{1,0:T(8,128)(2,1)}, u32[]{:S(2)}) copy-start(bf16[512,256]{1,0:T(8,128)(2,1)} %factor.1) | copy-start | bytes 786436
  2.6 1.0 %copy-start.2 = (bf16[512,512]{1,0:T(8,128)(2,1)S(1)}, bf16[512,512]{1,0:T(8,128)(2,1)}, u32[]{:S(2)}) copy-start(bf16[512,512]{1,0:T(8,128)(2,1)} %v_h.1) | copy-start | bytes 1572868
  3.7 1.0 %copy-start.3 = (bf16[512,512]{1,0:T(8,128)(2,1)S(1)}, bf16[512,512]{1,0:T(8,128)(2,1)}, u32[]{:S(2)}) copy-start(bf16[512,512]{1,0:T(8,128)(2,1)} %g_h.1) | copy-start | bytes 1572868
  4.7 0.8 %copy-start.4 = (f32[64,256]{1,0:T(8,128)S(1)}, f32[64,256]{1,0:T(8,128)}, u32[]{:S(2)}) copy-start(f32[64,256]{1,0:T(8,128)} %fm.1) | copy-start | bytes 196612
  5.6 0.8 %copy-start.5 = (f32[64,256]{1,0:T(8,128)S(1)}, f32[64,256]{1,0:T(8,128)}, u32[]{:S(2)}) copy-start(f32[64,256]{1,0:T(8,128)} %sm.1) | copy-start | bytes 196612
  6.4 0.9 %copy-start.6 = (bf16[512,256]{1,0:T(8,128)(2,1)S(1)}, bf16[512,256]{1,0:T(8,128)(2,1)}, u32[]{:S(2)}) copy-start(bf16[512,256]{1,0:T(8,128)(2,1)} %q_h.1) | copy-start | bytes 786436
  7.3 0.9 %copy-start.7 = (bf16[512,256]{1,0:T(8,128)(2,1)S(1)}, bf16[512,256]{1,0:T(8,128)(2,1)}, u32[]{:S(2)}) copy-start(bf16[512,256]{1,0:T(8,128)(2,1)} %k_h.1) | copy-start | bytes 786436
  8.3 0.7 %copy-start.8 = (f32[4]{0:T(128)S(1)}, f32[4]{0:T(128)}, u32[]{:S(2)}) copy-start(f32[4]{0:T(128)} %scale_ref.1) | copy-start | bytes 52

commit v2 on v1

--- a/solution.py
+++ b/solution.py
@@ -54,10 +54,10 @@
 
 def main_kernel(
     fs, rep, tp, head_width,
-    scale_ref, tok_h, q_h, k_h, v_h, g_h, factor_h, weight_h, first_h, second_h,
+    scale_h, tok_h, q_h, k_h, v_h, g_h, factor_h, weight_h, first_h, second_h,
     fac, wbf, dirs, proj, sq_out,
-    tok, q_v, k_v, v_v, g_v, wq, wsend, fm, sm, acc, kgb, red, psend, precv, sq_own, sq_in,
-    ld, fac_s, fac_r, par_s, par_r, w_s, w_r, wf_s, wf_r, pc_s, pc_r, dr_s, dr_r, pj_s, pj_r, sq_s, sq_r,
+    scale_ref, tok, q_v, k_v, v_v, g_v, wq, wsend, fm, sm, acc, kgb, red, psend, precv, sq_own, sq_in,
+    ld, fac_s, fac_r, fq_s, fq_r, fr_s, fr_r, par_s, par_r, w_s, w_r, wf_s, wf_r, pc_s, pc_r, dr_s, dr_r, pj_s, pj_r, sq_s, sq_r,
 ):
     n = fs * rep
     z, r, c = lax.axis_index("fs"), lax.axis_index("rep"), lax.axis_index("tp")
@@ -102,7 +102,7 @@
         for i, (src, dst) in enumerate(
             [
                 (factor_h, fac.at[z]), (weight_h.at[r], wq), (q_h, q_v), (k_h, k_v), (v_h, v_v), (g_h, g_v),
-                (tok_h, tok), (first_h.at[r], fm), (second_h.at[r], sm),
+                (scale_h, scale_ref), (tok_h, tok), (first_h.at[r], fm), (second_h.at[r], sm),
             ]
         )
     ]
@@ -114,12 +114,41 @@
     pl.semaphore_wait(barrier, n)
 
     def fac_copy(slot, sem, to):
-        part = fac.at[slot, :, my_cols]
+        part = fac.at[slot, pl.ds(0, direct), my_cols]
         return remote(part, part, fac_s.at[sem], fac_r.at[slot], fs_dev(to))
+
+    share = fac.shape[1] // (2 * rep)
+    share = share if share % 16 == 0 else 0
+    direct = fac.shape[1] - share * rep
+
+    def share_rows(lane):
+        return pl.ds(pl.multiple_of(direct + lane * share, 16), share)
+
+    def fq_copy(slot, sem, to):
+        part = fac.at[slot, share_rows(r), my_cols]
+        return remote(part, part, fq_s.at[sem], fq_r.at[slot], fs_dev(to))
+
+    def fr_copy(slot, lane, sem, to):
+        part = fac.at[slot, share_rows(lane), my_cols]
+        return remote(part, part, fr_s.at[slot, sem], fr_r.at[slot, lane], rep_dev(to))
+
+    def relay_fac(d):
+        src = lax.rem(z + d, fs)
+        fq_copy(src, d, src).wait_recv()
+        each(rep, lambda k: fr_copy(src, r, k, lax.rem(r + k, rep)).start())
+
+    def wait_fac_relay(src):
+        def inner(k):
+            lane = lax.rem(r + k, rep)
+            fr_copy(src, lane, k, lane).wait_recv()
+
+        each(rep, inner)
 
     def send_fac(d):
         fac_copy(z, d, lax.rem(z + d, fs)).start()
 
+    if share:
+        each(fs, lambda d: fq_copy(z, d, lax.rem(z + d, fs)).start())
     each(fs, send_fac)
 
     def w_copy(slot, sem, to):
@@ -130,11 +159,13 @@
 
     each(fs, send_w)
 
-    for i in range(2, 6):
+    for i in range(2, 7):
         loads[i].wait()
     for pair in range(q_v.shape[1] // LANES):
         attention_pair(pair, q_v, k_v, v_v, g_v, scale_ref, acc, kgb, head_width)
-    for i in range(6, 9):
+        if pair == 0 and share:
+            each(fs, relay_fac)
+    for i in range(7, 10):
         loads[i].wait()
 
     by_shard = fac.shape[1] % LANES == 0
@@ -152,6 +183,8 @@
     def forward_fac(d):
         src = lax.rem(z + d, fs)
         fac_copy(src, d, src).wait_recv()
+        if share:
+            wait_fac_relay(src)
         par_copy(src, my_cols).start()
 
     each(fs, forward_fac)
@@ -247,6 +280,9 @@
     def wait_sends_fs(d):
         src = lax.rem(z + d, fs)
         fac_copy(z, d, src).wait_send()
+        if share:
+            fq_copy(z, d, src).wait_send()
+            each(rep, lambda k: fr_copy(src, r, k, lax.rem(r + k, rep)).wait_send())
         w_copy(z, d, src).wait_send()
         par_copy(src, my_cols).wait_send()
         each(rep, lambda k: wf_copy(src, r, k, lax.rem(r + k, rep)).wait_send())
@@ -298,7 +334,7 @@
     piece = own_rows // rep
     w_rows = rows // rep
     f32, bf16 = jnp.float32, jnp.bfloat16
-    any_spec = pl.BlockSpec(memory_space=pl.ANY)
+    hbm = pl.BlockSpec(memory_space=pltpu.HBM)
     vmem = pl.BlockSpec(memory_space=pltpu.VMEM)
     dma = pltpu.SemaphoreType.DMA
     fac, wbf, dirs, proj, sq = pl.pallas_call(
@@ -310,9 +346,10 @@
             jax.ShapeDtypeStruct((rep, piece, width), f32),
             jax.ShapeDtypeStruct((8, LANES), f32),
         ),
-        in_specs=[pl.BlockSpec(memory_space=pltpu.SMEM)] + [any_spec] * 9,
+        in_specs=[hbm] * 10,
         out_specs=(vmem,) * 5,
         scratch_shapes=[
+            pltpu.SMEM(second_scale.shape, f32),
             pltpu.VMEM(tokens_in.shape, bf16),
             pltpu.VMEM(query_two.shape, bf16),
             pltpu.VMEM(key_two.shape, bf16),
@@ -329,8 +366,9 @@
             pltpu.VMEM((n, piece, width), bf16),
             pltpu.VMEM((8, LANES), f32),
             pltpu.VMEM((8, LANES), f32),
-            dma((9,)),
+            dma((10,)),
             dma((fs,)), dma((fs,)),
+            dma((fs,)), dma((fs,)), dma((fs, rep)), dma((fs, rep)),
             dma((fs,)), dma((fs,)),
             dma((fs,)), dma((fs,)),
             dma((fs, rep)), dma((fs, rep)),
@@ -340,7 +378,7 @@
             dma, dma,
         ],
         compiler_params=pltpu.CompilerParams(
-            collective_id=0, has_side_effects=True, vmem_limit_bytes=48 * 1024 * 1024
+            collective_id=0, has_side_effects=True, vmem_limit_bytes=60 * 1024 * 1024
         ),
         name="main_kernel",
     )(
@@ -360,7 +398,7 @@
         ),
         in_specs=[vmem] * 9,
         out_specs=(vmem,) * 5,
-        compiler_params=pltpu.CompilerParams(vmem_limit_bytes=32 * 1024 * 1024),
+        compiler_params=pltpu.CompilerParams(vmem_limit_bytes=60 * 1024 * 1024),
         name="end_kernel",
     )(
         sq, factor, dirs.reshape(n * piece, width), fac.reshape(fs * rows, rank),

time: 49.9 us -> 40.1 us (0.80); the launches traced: 48.9 us -> 39.9 us
  local copies, waits for them, and re-layouts: 8.3 us -> 0 us
  Pallas kernels: 39.9 us -> 39.3 us
    unnamed x18 -> x0, local copies, waits for them, and re-layouts: 8.3 us -> none
    pallas_call x1, Pallas kernels: 38.3 us -> 35.8 us  [on_device(): pl.pallas_call(functools.partial(main_kernel, fs, rep, tp, head_width), o...]
    pallas_call x1, Pallas kernels: 1.68 us -> 3.53 us  [on_device(): pl.pallas_call(functools.partial(end_kernel, fs, float(rank * width * tp)...]
where the time goes in v2:
time: 40.1 us; the launch traced here: 39.9 us
  Pallas kernels  39.3 us (98%)
  between operations  0.64 us (2%)
    pallas_call x1, Pallas kernels, on_device(): pl.pallas_call(functools.partial(main_kernel, fs, rep, tp, head_width), o...  35.8 us
    pallas_call x1, Pallas kernels, on_device(): pl.pallas_call(functools.partial(end_kernel, fs, float(rank * width * tp)...  3.53 us

profile of v2, /device:TPU:9, one launch (start us, length us, event | category | flops | bytes accessed | tf_op | source)
XLA Modules:
  0.0 39.9 jit_solution(9511332666608372504)
XLA Ops:
  0.6 35.8 %main_kernel.1 = (bf16[4,512,256]{2,1,0:T(8,128)(2,1)}, bf16[4,4,128,256]{3,2,1,0:T(8,128)(2,1)}, bf16[16,16,256]{2,1,0:T(8,128)(2,1)}, f32[4,16,256]{2,1,0:T(8,128)}, f32[8,128]{1,0:T(8,128)}) custom-call(f32[4]{0:T(128)} %scale_h.1, bf16[512,2048]{1,0:T(8,128)(2,1)} %tok_h.1, bf16[512,256]{1,0:T(8,128)(2,1)} %q_h.1, bf16[512,256]{1,0:T(8,128)(2,1)} %k_h.1, ...), custom_call_target="tpu_custom_call" | custom-call | tf_op jit(solution)/shard_map/main_kernel/pallas_call | solution.py:340
  36.4 3.5 %end_kernel.1 = (f32[512,256]{1,0:T(8,128)}, bf16[2048,256]{1,0:T(8,128)(2,1)}, f32[512,256]{1,0:T(8,128)}, f32[64,256]{1,0:T(8,128)}, f32[64,256]{1,0:T(8,128)}) custom-call(f32[8,128]{1,0:T(8,128)} %get-tuple-element.10.sq, bf16[512,256]{1,0:T(8,128)(2,1)} %factor.1, bf16[256,256]{1,0:T(8,128)(2,1)} %bitcast.12, bf16[2048,256]{1,0:T(8,128)(2,1)} %bitcast.8, ...), custom_call_target="tpu_custom_call" | custom-call | tf_op jit(solution)/shard_map/end_kernel/pallas_call | solution.py:390

commit v3 on v2

--- a/solution.py
+++ b/solution.py
@@ -55,8 +55,8 @@
 def main_kernel(
     fs, rep, tp, head_width,
     scale_h, tok_h, q_h, k_h, v_h, g_h, factor_h, weight_h, first_h, second_h,
-    fac, wbf, dirs, proj, sq_out,
-    scale_ref, tok, q_v, k_v, v_v, g_v, wq, wsend, fm, sm, acc, kgb, red, psend, precv, sq_own, sq_in,
+    fac_o, wbf_o, dirs, proj, sq_out,
+    fac, wbf, scale_ref, tok, q_v, k_v, v_v, g_v, wq, wsend, fm, sm, acc, kgb, red, psend, precv, sq_own, sq_in,
     ld, fac_s, fac_r, fq_s, fq_r, fr_s, fr_r, par_s, par_r, w_s, w_r, wf_s, wf_r, pc_s, pc_r, dr_s, dr_r, pj_s, pj_r, sq_s, sq_r,
 ):
     n = fs * rep
@@ -117,7 +117,7 @@
         part = fac.at[slot, pl.ds(0, direct), my_cols]
         return remote(part, part, fac_s.at[sem], fac_r.at[slot], fs_dev(to))
 
-    share = fac.shape[1] // (2 * rep)
+    share = (fac.shape[1] * 3) // (4 * rep)
     share = share if share % 16 == 0 else 0
     direct = fac.shape[1] - share * rep
 
@@ -200,6 +200,8 @@
         whole = jnp.concatenate([fac[j] for j in range(fs)], axis=0)
         red[...] = jnp.dot(tok[...], whole, preferred_element_type=jnp.float32)
 
+    fac_out = pltpu.make_async_copy(fac, fac_o, ld.at[10])
+    fac_out.start()
     partial = lax.dot_general(
         red[...].astype(jnp.bfloat16), kgb[...], TN, preferred_element_type=jnp.float32
     )
@@ -277,6 +279,10 @@
 
     each(fs, wait_relay)
 
+    wbf[z] = jnp.zeros(wbf.shape[1:], jnp.bfloat16)
+    wbf_out = pltpu.make_async_copy(wbf, wbf_o, ld.at[11])
+    wbf_out.start()
+
     def wait_sends_fs(d):
         src = lax.rem(z + d, fs)
         fac_copy(z, d, src).wait_send()
@@ -297,6 +303,8 @@
     each(n, wait_sends_all)
     each(rep, lambda d: pj_copy(r, d, lax.rem(r + d, rep)).wait_send())
     sq_copy.wait()
+    fac_out.wait()
+    wbf_out.wait()
     sq_out[...] = sq_own[...] + sq_in[...]
 
 
@@ -347,8 +355,10 @@
             jax.ShapeDtypeStruct((8, LANES), f32),
         ),
         in_specs=[hbm] * 10,
-        out_specs=(vmem,) * 5,
+        out_specs=(hbm, hbm, vmem, vmem, vmem),
         scratch_shapes=[
+            pltpu.VMEM((fs, rows, rank), bf16),
+            pltpu.VMEM((fs, rep, w_rows, width), bf16),
             pltpu.SMEM(second_scale.shape, f32),
             pltpu.VMEM(tokens_in.shape, bf16),
             pltpu.VMEM(query_two.shape, bf16),
@@ -366,7 +376,7 @@
             pltpu.VMEM((n, piece, width), bf16),
             pltpu.VMEM((8, LANES), f32),
             pltpu.VMEM((8, LANES), f32),
-            dma((10,)),
+            dma((12,)),
             dma((fs,)), dma((fs,)),
             dma((fs,)), dma((fs,)), dma((fs, rep)), dma((fs, rep)),
             dma((fs,)), dma((fs,)),

time: 40.1 us -> 39.1 us (0.975)
  Pallas kernels: 39.3 us -> 38.3 us
    pallas_call x1, Pallas kernels: 35.8 us -> 34.8 us  [on_device(): pl.pallas_call(functools.partial(main_kernel, fs, rep, tp, head_width), o...]
where the time goes in v3:
time: 39.1 us; the launch traced here: 38.9 us
  Pallas kernels  38.3 us (98%)
  between operations  0.64 us (2%)
    pallas_call x1, Pallas kernels, on_device(): pl.pallas_call(functools.partial(main_kernel, fs, rep, tp, head_width), o...  34.8 us
    pallas_call x1, Pallas kernels, on_device(): pl.pallas_call(functools.partial(end_kernel, fs, float(rank * width * tp)...  3.53 us

profile of v3, /device:TPU:9, one launch (start us, length us, event | category | flops | bytes accessed | tf_op | source)
XLA Modules:
  0.0 38.9 jit_solution(10892286674573797626)
XLA Ops:
  0.6 34.8 %main_kernel.1 = (bf16[4,512,256]{2,1,0:T(8,128)(2,1)}, bf16[4,4,128,256]{3,2,1,0:T(8,128)(2,1)}, bf16[16,16,256]{2,1,0:T(8,128)(2,1)}, f32[4,16,256]{2,1,0:T(8,128)}, f32[8,128]{1,0:T(8,128)}) custom-call(f32[4]{0:T(128)} %scale_h.1, bf16[512,2048]{1,0:T(8,128)(2,1)} %tok_h.1, bf16[512,256]{1,0:T(8,128)(2,1)} %q_h.1, bf16[512,256]{1,0:T(8,128)(2,1)} %k_h.1, ...), custom_call_target="tpu_custom_call" | custom-call | tf_op jit(solution)/shard_map/main_kernel/pallas_call | solution.py:348
  35.4 3.5 %end_kernel.1 = (f32[512,256]{1,0:T(8,128)}, bf16[2048,256]{1,0:T(8,128)(2,1)}, f32[512,256]{1,0:T(8,128)}, f32[64,256]{1,0:T(8,128)}, f32[64,256]{1,0:T(8,128)}) custom-call(f32[8,128]{1,0:T(8,128)} %get-tuple-element.10.sq, bf16[512,256]{1,0:T(8,128)(2,1)} %factor.1, bf16[256,256]{1,0:T(8,128)(2,1)} %bitcast.12, bf16[2048,256]{1,0:T(8,128)(2,1)} %bitcast.8, ...), custom_call_target="tpu_custom_call" | custom-call | tf_op jit(solution)/shard_map/end_kernel/pallas_call | solution.py:400
